TPU v7x, 32 devices: a whole 2x2x4 slice. The times are simulated.
32 devices in a mesh: grp: 2 (over y), ep: 8 (over z, x), tp: 2 (over core).
Axes of the slice: x: 2, y: 2, z: 4, core: 2. Of those that a mesh axis runs over, the one named last changes fastest.
Arguments:
- tokens: bfloat16 [4096, 2048], P(('grp', 'ep', 'tp')), parts along dimension 0, may hold values from -6 to 6
- expert_ids: int32 [4096, 4], P(('grp', 'ep', 'tp')), parts along dimension 0, may hold values from 0 to 15, all different within a row; in each aligned block of 128 rows (0 to 127, 128 to 255, ...) at most 48 rows name the same one
- gate_weights: float32 [4096, 4], P(('grp', 'ep', 'tp')), parts along dimension 0, may hold values from 0.1 to 1
- norm_gain: float32 [2048], replicated, may hold values from 0.1 to 1.9
- expert_gate: bfloat16 [16, 2048, 512], P(('ep', 'tp')), may hold values from -0.125 to 0.125
- expert_up: bfloat16 [16, 2048, 512], P(('ep', 'tp')), may hold values from -0.125 to 0.125
- expert_down: bfloat16 [16, 512, 2048], P(('ep', 'tp'))
- shared_gate: bfloat16 [2048, 512], P(None, 'tp'), may hold values from -0.125 to 0.125
- shared_up: bfloat16 [2048, 512], P(None, 'tp'), may hold values from -0.125 to 0.125
- shared_down: bfloat16 [512, 2048], P('tp')
- out_gain: float32 [2048], replicated, may hold values from 0.1 to 1.9
Outputs:
- layer_out: bfloat16 [4096, 2048], P(('grp', 'ep'), 'tp'), parts along dimension 0
There are 2 independent parts, one for each index of `grp`. A program takes and returns all parts, laid end to end along the dimension named above; an argument that names none is the same for every part. Nothing has to cross between parts.
Inputs may be any that keep to these rules, and one draw needn't show every extreme that they name: `expert_ids`: each row names 4 different experts. Among the 128 rows of one device (aligned blocks of rows), no expert is named more than 48 times, and in every draw some expert is named exactly 48 times by some device.
All inputs are finite; a program needn't handle non-finite values.
Results may differ from a plain program's by a relative error of at most 0.0085.
Values may be sent and summed in bfloat16 or wider, within the bound.
A program may use at most 64 MiB of HBM per device.

v0:
```python
import functools

import jax
import jax.numpy as jnp
from jax import lax
from jax.experimental import pallas as pl
from jax.experimental.pallas import tpu as pltpu
from jax.sharding import PartitionSpec as P

MESH = pl.DeviceIdType.MESH
PARTS = 4
F32 = jnp.float32
BF16 = jnp.bfloat16


def ring_kernel(
    n,
    ids_ref,
    gates_ref,
    tok_hbm,
    gain_ref,
    out_gain_ref,
    eg_hbm,
    eu_hbm,
    ed_hbm,
    sg_hbm,
    su_hbm,
    sd_hbm,
    out_ref,
    tok,
    own_x,
    own_w,
    rx,
    wrx,
    wg,
    wu,
    wd_mine,
    wd_other,
    sg,
    su,
    sd_mine,
    sd_other,
    kept,
    psend,
    prx,
    home,
    home_send,
    home_rx,
    rs_send,
    rs_rx,
    sq_send,
    sq_rx,
    tok_sem,
    load_sem,
    ag_ssem,
    ag_rsem,
    w_ssem,
    w_rsem,
    pag_ssem,
    pag_rsem,
    pw_ssem,
    pw_rsem,
    ox_ssem,
    ox_rsem,
    p_ssem,
    p_rsem,
    h_ssem,
    h_rsem,
    rs_ssem,
    rs_rsem,
    sq_ssem,
    sq_rsem,
):
    per = 2 * PARTS
    slots = (n - 1) * PARTS
    rows, width = tok.shape
    chunk = rows // per
    cols = width // 2
    topk = ids_ref.shape[0]
    experts = own_w.shape[1]
    turn = n // 2
    ep = lax.axis_index("ep")
    c = lax.axis_index("tp")
    oc = 1 - c
    x = ep % 2
    z = ep // 2
    pos = z * (1 - x) + (n - 1 - z) * x

    def at(p):
        q = p // turn
        return 2 * p * (1 - q) + (2 * (n - 1 - p) + 1) * q

    toward = (at((pos + 1) % n), at((pos + n - 1) % n))
    mine = ep * 2 + c

    barrier = pltpu.get_barrier_semaphore()
    for e in toward:
        pl.semaphore_signal(barrier, inc=1, device_id={"ep": e, "tp": c}, device_id_type=MESH)
    pl.semaphore_signal(barrier, inc=1, device_id={"ep": ep, "tp": oc}, device_id_type=MESH)

    tok_loads = []
    for j, k in enumerate([k for s in range(PARTS) for k in (s, s + PARTS)]):
        part = pl.ds(k * chunk, chunk)
        tok_loads.append(pltpu.make_async_copy(tok_hbm.at[part], tok.at[part], tok_sem.at[j]))
        tok_loads[-1].start()

    lo, hi = pl.ds(pl.multiple_of(c * cols, cols), cols), pl.ds(pl.multiple_of(oc * cols, cols), cols)
    loads = [
        (eg_hbm.at[0], wg),
        (eu_hbm.at[0], wu),
        (ed_hbm.at[0, :, hi], wd_other),
        (ed_hbm.at[0, :, lo], wd_mine),
        (sg_hbm, sg),
        (su_hbm, su),
        (sd_hbm.at[:, hi], sd_other),
        (sd_hbm.at[:, lo], sd_mine),
    ]
    loads = [pltpu.make_async_copy(s, d, load_sem.at[i]) for i, (s, d) in enumerate(loads)]
    for load in loads:
        load.start()

    expert = lax.broadcasted_iota(jnp.int32, (experts, rows), 0)
    dense = jnp.zeros((experts, rows), F32)
    for k in range(topk):
        dense += jnp.where(ids_ref[k : k + 1, :] == expert, gates_ref[k : k + 1, :], 0.0)
    own_w[c] = dense

    def remote(src, dst, ssem, rsem, e, core):
        return pltpu.make_async_remote_copy(
            src_ref=src,
            dst_ref=dst,
            send_sem=ssem,
            recv_sem=rsem,
            device_id={"ep": e, "tp": core},
            device_id_type=MESH,
        )

    def ag(s, d, src):
        return remote(src, rx.at[s, d, c], ag_ssem.at[s, d], ag_rsem.at[s, d], toward[d], c)

    def agw(i, d, src):
        return remote(src, wrx.at[i, d, c], w_ssem.at[i, d], w_rsem.at[i, d], toward[d], c)

    def pag(s, d, core):
        return remote(
            rx.at[s, d, core], rx.at[s, d, core], pag_ssem.at[s, d], pag_rsem.at[s, d], ep, oc
        )

    def pagw(i, d, core):
        return remote(
            wrx.at[i, d, core], wrx.at[i, d, core], pw_ssem.at[i, d], pw_rsem.at[i, d], ep, oc
        )

    def place(s, d):
        return (s + d * PARTS) % per

    def own_chunk(s, d):
        return own_x.at[c, pl.ds(place(s, d) * chunk, chunk)]

    def normalise(k):
        part = pl.ds(k * chunk, chunk)
        values = tok[part, :].astype(F32)
        scale = lax.rsqrt(jnp.mean(values * values, axis=1, keepdims=True) + 1e-06)
        own_x[c, part, :] = (values * scale * gain_ref[...]).astype(BF16)

    for s in range(PARTS):
        for d in range(2):
            tok_loads[2 * s + d].wait()
            normalise(s + d * PARTS)
        if s == 0:
            pl.semaphore_wait(barrier, 3)
            for d in range(2):
                agw(0, d, own_w.at[c]).start()
        for d in range(2):
            ag(s, d, own_chunk(s, d)).start()
    for s in range(PARTS, per):
        for d in range(2):
            ag(s, d, own_chunk(s, d)).start()
    home_copies = (
        lambda core: remote(own_x.at[core], own_x.at[core], ox_ssem.at[0], ox_rsem.at[0], ep, oc),
        lambda core: remote(own_w.at[core], own_w.at[core], ox_ssem.at[1], ox_rsem.at[1], ep, oc),
    )
    for copy in home_copies:
        copy(c).start()

    def relay(s):
        i = s // per
        first = s % per == 0
        for d in range(2):
            ag(s, d, rx.at[s, d, c]).wait_recv()

            @pl.when(s + per < slots)
            def _():
                ag(s + per, d, rx.at[s, d, c]).start()

            pag(s, d, c).start()

            @pl.when(first)
            def _():
                agw(i, d, wrx.at[i, d, c]).wait_recv()

                @pl.when(s + per < slots)
                def _():
                    agw(i + 1, d, wrx.at[i, d, c]).start()

                pagw(i, d, c).start()

    relay(0)

    def silu_mul(g, u):
        return (g / (1.0 + jnp.exp(-g)) * u).astype(BF16)

    def dot(a, b):
        return jnp.dot(a, b, preferred_element_type=F32)

    def column(row, offset, count):
        r = lax.broadcasted_iota(jnp.int32, (count, rows), 0) + offset
        q = lax.broadcasted_iota(jnp.int32, (count, rows), 1)
        return jnp.sum(jnp.where(r == q, row, 0.0), axis=1, keepdims=True)

    for load in loads:
        load.wait()
    for copy in home_copies:
        copy(oc).wait_recv()

    xs = own_x[...].reshape(2 * rows, width)
    hidden = silu_mul(dot(xs, wg[...]), dot(xs, wu[...]))
    shared = silu_mul(dot(xs, sg[...]), dot(xs, su[...]))
    weight = jnp.concatenate(
        [column(own_w[k, pl.ds(mine, 1), :], 0, rows) for k in range(2)], axis=0
    )
    home_send[...] = dot(hidden, wd_other[...]) * weight + dot(shared, sd_other[...])
    home[...] = dot(hidden, wd_mine[...]) * weight + dot(shared, sd_mine[...])
    home_copy = remote(home_send, home_rx, h_ssem.at[0], h_rsem.at[0], ep, oc)
    home_copy.start()

    def partner(s):
        return remote(psend.at[s], prx.at[s], p_ssem.at[s], p_rsem.at[s], ep, oc)

    def work(s):
        i = s // per
        first = s % per == 0
        for d in range(2):
            pag(s, d, oc).wait_recv()

            @pl.when(first)
            def _():
                pagw(i, d, oc).wait_recv()

        weight = jnp.concatenate(
            [
                column(
                    wrx[i, d, k, pl.ds(mine, 1), :],
                    place(s, d) * chunk,
                    chunk,
                )
                for d in range(2)
                for k in range(2)
            ],
            axis=0,
        )
        xs = rx[s].reshape(4 * chunk, width)
        hidden = silu_mul(dot(xs, wg[...]), dot(xs, wu[...]))
        psend[s] = (dot(hidden, wd_other[...]) * weight).astype(BF16)
        kept[s] = dot(hidden, wd_mine[...]) * weight
        partner(s).start()

    def back(s, d):
        return remote(
            rs_send.at[s, d], rs_rx.at[s, d], rs_ssem.at[s, d], rs_rsem.at[s, d], toward[1 - d], c
        )

    def give(s, further):
        partner(s).wait_recv()
        for d in range(2):
            part = pl.ds(d * 2 * chunk, 2 * chunk)
            total = kept[s, part, :] + prx[s, part, :].astype(F32)
            if further:
                back(s + per, d).wait_recv()
                total += rs_rx[s + per, d].astype(F32)
            rs_send[s, d] = total.astype(BF16)
            back(s, d).start()

    def step(s, _):
        relay(s + 1)
        work(s)
        return 0

    lax.fori_loop(0, slots - per, step, 0)
    for s in range(slots - per, slots):
        if s + 1 < slots:
            lax.fori_loop(s, s + 1, step, 0)
        else:
            work(s)
        if s > slots - per:
            give(s - 1, False)
    give(slots - 1, False)
    home_copy.wait_recv()
    home[...] += home_rx[...]
    order = [s for k in range(slots - 2 * per, -1, -per) for s in range(k, k + per)]
    for s in order + list(range(slots % per)):
        give(s, True)

    def squares(s):
        return remote(sq_send.at[s], sq_rx.at[s], sq_ssem.at[s], sq_rsem.at[s], ep, oc)

    def home_rows(s, d, k):
        return pl.ds(k * rows + place(s, d) * chunk, chunk)

    for s in [*range(PARTS, per), *range(PARTS)]:
        for d in range(2):
            back(s, d).wait_recv()
            for k in range(2):
                part = home_rows(s, d, k)
                total = home[part, :] + rs_rx[s, d, pl.ds(k * chunk, chunk), :].astype(F32)
                if s < PARTS:
                    total = total.astype(BF16).astype(F32)
                    sq = jnp.sum(total * total, axis=1, keepdims=True)
                    sq_send[s, pl.ds((2 * d + k) * chunk, chunk), :] = jnp.broadcast_to(
                        sq, (chunk, 128)
                    )
                home[part, :] = total
        if s < PARTS:
            squares(s).start()
    for s in range(PARTS):
        squares(s).wait_recv()
        final = lax.rsqrt((sq_send[s] + sq_rx[s])[:, :1] / width + 1e-06)
        for d in range(2):
            for k in range(2):
                part = home_rows(s, d, k)
                at_k = (2 * d + k) * chunk
                out_ref[part, :] = (
                    home[part, :] * final[at_k : at_k + chunk] * out_gain_ref[c]
                ).astype(BF16)

    for d in range(2):
        for s in range(slots):
            ag(s, d, rx.at[s, d, c]).wait_send()
            pag(s, d, c).wait_send()
            back(s, d).wait_send()
        for i in range(turn):
            agw(i, d, wrx.at[i, d, c]).wait_send()
            pagw(i, d, c).wait_send()
    for s in range(slots):
        partner(s).wait_send()
    for copy in home_copies:
        copy(c).wait_send()
    home_copy.wait_send()
    for s in range(PARTS):
        squares(s).wait_send()


def ring_local(
    n,
    tokens,
    expert_ids,
    gate_weights,
    norm_gain,
    expert_gate,
    expert_up,
    expert_down,
    shared_gate,
    shared_up,
    shared_down,
    out_gain,
):
    rows, width = tokens.shape
    ff = expert_gate.shape[2]
    sh = shared_gate.shape[1]
    cols = width // 2
    slots, turn = (n - 1) * PARTS, n // 2
    chunk = rows // (2 * PARTS)
    experts = 2 * n * expert_gate.shape[0]
    dma = pltpu.SemaphoreType.DMA
    vmem = pl.BlockSpec(memory_space=pltpu.VMEM)
    hbm = pl.BlockSpec(memory_space=pl.ANY)
    return pl.pallas_call(
        functools.partial(ring_kernel, n),
        out_shape=pltpu.VMEM((2 * rows, cols), BF16),
        in_specs=[vmem] * 2 + [hbm] + [vmem] * 2 + [hbm] * 6,
        out_specs=vmem,
        scratch_shapes=[
            pltpu.VMEM((rows, width), BF16),
            pltpu.VMEM((2, rows, width), BF16),
            pltpu.VMEM((2, experts, rows), F32),
            pltpu.VMEM((slots, 2, 2, chunk, width), BF16),
            pltpu.VMEM((turn, 2, 2, experts, rows), F32),
            pltpu.VMEM((width, ff), BF16),
            pltpu.VMEM((width, ff), BF16),
            pltpu.VMEM((ff, cols), BF16),
            pltpu.VMEM((ff, cols), BF16),
            pltpu.VMEM((width, sh), BF16),
            pltpu.VMEM((width, sh), BF16),
            pltpu.VMEM((sh, cols), BF16),
            pltpu.VMEM((sh, cols), BF16),
            pltpu.VMEM((slots, 4 * chunk, cols), F32),
            pltpu.VMEM((slots, 4 * chunk, cols), BF16),
            pltpu.VMEM((slots, 4 * chunk, cols), BF16),
            pltpu.VMEM((2 * rows, cols), F32),
            pltpu.VMEM((2 * rows, cols), F32),
            pltpu.VMEM((2 * rows, cols), F32),
            pltpu.VMEM((slots, 2, 2 * chunk, cols), BF16),
            pltpu.VMEM((slots, 2, 2 * chunk, cols), BF16),
            pltpu.VMEM((PARTS, 4 * chunk, 128), F32),
            pltpu.VMEM((PARTS, 4 * chunk, 128), F32),
            dma((2 * PARTS,)),
            dma((8,)),
            dma((slots, 2)),
            dma((slots, 2)),
            dma((turn, 2)),
            dma((turn, 2)),
            dma((slots, 2)),
            dma((slots, 2)),
            dma((turn, 2)),
            dma((turn, 2)),
            dma((2,)),
            dma((2,)),
            dma((slots,)),
            dma((slots,)),
            dma((1,)),
            dma((1,)),
            dma((slots, 2)),
            dma((slots, 2)),
            dma((PARTS,)),
            dma((PARTS,)),
        ],
        compiler_params=pltpu.CompilerParams(
            collective_id=0, has_side_effects=True, vmem_limit_bytes=60 * 1024 * 1024
        ),
    )(
        expert_ids.T,
        gate_weights.T,
        tokens,
        norm_gain.reshape(1, width),
        out_gain.reshape(2, 1, cols),
        expert_gate,
        expert_up,
        expert_down,
        shared_gate,
        shared_up,
        shared_down,
    )


TOPK = 4


def expert_work(received, expert_gate, expert_up, expert_down):
    gate = jnp.einsum("slcd,ldf->slcf", received, expert_gate, preferred_element_type=jnp.float32)
    upper = jnp.einsum("slcd,ldf->slcf", received, expert_up, preferred_element_type=jnp.float32)
    hidden = (jax.nn.silu(gate) * upper).astype(jnp.bfloat16)
    return jnp.einsum(
        "slcf,lfd->slcd", hidden, expert_down, preferred_element_type=jnp.float32
    ).astype(jnp.bfloat16)


def local(
    tokens,
    expert_ids,
    gate_weights,
    norm_gain,
    expert_gate,
    expert_up,
    expert_down,
    shared_gate,
    shared_up,
    shared_down,
    out_gain,
):
    local_rows = tokens.shape[0]
    width = tokens.shape[1]
    ep_count = lax.axis_size("ep")
    tp_count = lax.axis_size("tp")
    device_count = ep_count * tp_count
    local_experts = expert_gate.shape[0]
    expert_count = device_count * local_experts
    capacity = 3 * local_rows * TOPK // (2 * expert_count)
    values = tokens.astype(jnp.float32)
    scale = lax.rsqrt(jnp.mean(values * values, axis=1, keepdims=True) + 1e-06)
    normed = (values * scale * norm_gain).astype(jnp.bfloat16)
    flat_ids = expert_ids.reshape(-1)
    one_hot = (flat_ids[:, None] == jnp.arange(expert_count, dtype=jnp.int32)[None, :]).astype(
        jnp.int32
    )
    earlier = jnp.cumsum(one_hot, axis=0) - one_hot
    slot_index = jnp.sum(earlier * one_hot, axis=1)
    target = flat_ids * capacity + slot_index
    copy_rows = normed[jnp.arange(local_rows * TOPK, dtype=jnp.int32) // TOPK]
    outgoing = jnp.zeros((expert_count * capacity, width), jnp.bfloat16).at[target].set(copy_rows)
    sending = outgoing.reshape(device_count, local_experts * capacity, width)
    received = lax.all_to_all(sending, ("ep", "tp"), split_axis=0, concat_axis=0, tiled=True)
    received = received.reshape(device_count, local_experts, capacity, width)
    results = expert_work(received, expert_gate, expert_up, expert_down)
    results = results.reshape(device_count, local_experts * capacity, width)
    returned = lax.all_to_all(results, ("ep", "tp"), split_axis=0, concat_axis=0, tiled=True)
    returned = returned.reshape(expert_count * capacity, width)
    picked = returned[target].astype(jnp.float32).reshape(local_rows, TOPK, width)
    routed = jnp.sum(picked * gate_weights[:, :, None], axis=1)
    piece = lax.all_gather(normed, "tp", axis=0, tiled=True)
    gate = jnp.dot(piece, shared_gate, preferred_element_type=jnp.float32)
    upper = jnp.dot(piece, shared_up, preferred_element_type=jnp.float32)
    shared_hidden = (jax.nn.silu(gate) * upper).astype(jnp.bfloat16)
    shared_out = lax.psum_scatter(
        jnp.dot(shared_hidden, shared_down, preferred_element_type=jnp.float32),
        "tp",
        scatter_dimension=0,
        tiled=True,
    )
    mixed = (routed + shared_out).astype(jnp.bfloat16)
    mixed_values = mixed.astype(jnp.float32)
    final_scale = lax.rsqrt(jnp.mean(mixed_values * mixed_values, axis=1, keepdims=True) + 1e-06)
    normalized = (mixed_values * final_scale * out_gain).astype(jnp.bfloat16)
    return lax.all_to_all(normalized, "tp", split_axis=1, concat_axis=0, tiled=True)


def solution(mesh):
    in_specs = (
        P(("grp", "ep", "tp"), None),
        P(("grp", "ep", "tp"), None),
        P(("grp", "ep", "tp"), None),
        P(),
        P(("ep", "tp"), None, None),
        P(("ep", "tp"), None, None),
        P(("ep", "tp"), None, None),
        P(None, "tp"),
        P(None, "tp"),
        P("tp", None),
        P(),
    )
    out_specs = P(("grp", "ep"), "tp")
    n, tp = mesh.shape["ep"], mesh.shape["tp"]

    def run(*args):
        tokens, expert_gate = args[0], args[4]
        rows = tokens.shape[0] // mesh.size
        experts = expert_gate.shape[0]
        dense = experts == n * tp and experts <= 8 * args[1].shape[1]
        dense = dense and tp == 2 and n % 2 == 0 and n >= 4 and rows == 128
        body = functools.partial(ring_local, n) if dense else local
        return jax.shard_map(
            body, mesh=mesh, in_specs=in_specs, out_specs=out_specs, check_vma=False
        )(*args)

    return run
```

profile of v0, /device:TPU:9, one launch (start us, length us, event | category | flops | bytes accessed | tf_op | source)
XLA Modules:
  0.0 90.9 jit_solution(5196954780414286650)
XLA Ops:
  0.0 90.1 %shard_map.109 = bf16[256,1024]{1,0:T(8,128)(2,1)S(1)} custom-call(s32[4,128]{1,0:T(4,128)} %bitcast.6, f32[4,128]{1,0:T(4,128)} %bitcast.7, bf16[128,2048]{1,0:T(8,128)(2,1)} %tok_hbm.1, f32[1,2048]{1,0:T(1,128)} %bitcast.4, f32[2,1,1024]{2,1,0:T(1,128)} %bitcast.5, bf16[1,2048,512]{2,1,0:T(8,128)(2,1)} %eg_hbm.1, bf16[1,2048,512]{2,1,0:T(8,128)(2,1)} %eu_hbm.1, ...), custom_call_target="tpu_custom_call" | custom-call | tf_op jit(solution)/shard_map/pallas_call | solution.py:377
  90.1 0.8 copy.13
where the time goes:
time: 92 us; the launch traced here: 90.9 us
  Pallas kernels  90.1 us (98%)
    pallas_call x1, Pallas kernels, ring_local(): pl.pallas_call(functools.partial(ring_kernel, n), out_shape=pltpu.VMEM((2...  90.1 us

commit v1 on v0

v1 whole, which is shorter than its diff:
```python
import functools

import jax
import jax.numpy as jnp
from jax import lax
from jax.experimental import pallas as pl
from jax.experimental.pallas import tpu as pltpu
from jax.sharding import PartitionSpec as P

MESH = pl.DeviceIdType.MESH
CHUNKS = 4
BACKS = 4
F32 = jnp.float32
BF16 = jnp.bfloat16


def ladder_kernel(
    n,
    cap,
    ids_ref,
    gates_ref,
    tok_hbm,
    gain_ref,
    out_gain_ref,
    eg_hbm,
    eu_hbm,
    ed_hbm,
    sg_hbm,
    su_hbm,
    sd_hbm,
    out_ref,
    tok,
    xo,
    xl,
    meta,
    mall,
    stage,
    xr,
    wg,
    wu,
    wd,
    sg,
    su,
    sd,
    res,
    ret,
    pt,
    acc,
    rs_send,
    rs_rx,
    home,
    home_send,
    home_rx,
    sq_send,
    sq_rx,
    tok_sem,
    load_sem,
    own_ss,
    rail_ss,
    rail_rs,
    mown_ss,
    mrail_ss,
    mrail_rs,
    md_ss,
    md_rs,
    disp_ss,
    disp_rs,
    ret_ss,
    ret_rs,
    back_ss,
    back_rs,
    ox_ss,
    ox_rs,
    h_ss,
    h_rs,
    sq_ss,
    sq_rs,
):
    levels = n // 2
    rows, width = tok.shape
    cols = width // 2
    cw, rw = width // CHUNKS, cols // BACKS
    topk = ids_ref.shape[0]
    per = 4
    experts = levels * per
    ep = lax.axis_index("ep")
    c = lax.axis_index("tp")
    oc = 1 - c
    x = ep % 2
    z = ep // 2
    ox = 1 - x
    across = z * 2 + ox
    mine = 2 * x + c
    others = (2 * x + oc, 2 * ox + c, 2 * ox + oc)
    homes = ((ep, oc), (across, c), (across, oc))
    has = (z < levels - 1, z > 0)
    beside = (jnp.minimum(ep + 2, n - 1), jnp.maximum(ep - 2, 0))
    at_end = (z == 0) | (z == levels - 1)

    def signal(e, core):
        pl.semaphore_signal(barrier, inc=1, device_id={"ep": e, "tp": core}, device_id_type=MESH)

    barrier = pltpu.get_barrier_semaphore()
    for e, core in homes:
        signal(e, core)
    for d in range(2):

        @pl.when(has[d])
        def _():
            signal(beside[d], c)

    tok_load = pltpu.make_async_copy(tok_hbm, tok, tok_sem.at[0])
    tok_load.start()

    loads = [
        (sg_hbm, sg),
        (su_hbm, su),
        (sd_hbm.at[:, pl.ds(0, cols)], sd.at[0]),
        (sd_hbm.at[:, pl.ds(cols, cols)], sd.at[1]),
        (eg_hbm.at[0], wg),
        (eu_hbm.at[0], wu),
        (ed_hbm.at[0, :, pl.ds(0, cols)], wd.at[0]),
        (ed_hbm.at[0, :, pl.ds(cols, cols)], wd.at[1]),
    ]
    loads = [pltpu.make_async_copy(s, d, load_sem.at[i]) for i, (s, d) in enumerate(loads)]
    def remote(src, dst, ssem, rsem, e, core):
        return pltpu.make_async_remote_copy(
            src_ref=src,
            dst_ref=dst,
            send_sem=ssem,
            recv_sem=rsem,
            device_id={"ep": e, "tp": core},
            device_id_type=MESH,
        )

    def dot(a, b):
        return jnp.dot(a, b, preferred_element_type=F32)

    def cs(q):
        return pl.ds(q * cw, cw)

    def ss(s):
        return pl.ds(s * rw, rw)

    expert = lax.broadcasted_iota(jnp.int32, (experts, rows), 0)
    dense = jnp.zeros((experts, rows), F32)
    member = jnp.zeros((experts, rows), F32)
    for k in range(topk):
        hit = ids_ref[k : k + 1, :] == expert
        dense += jnp.where(hit, gates_ref[k : k + 1, :], 0.0)
        member += jnp.where(hit, 1.0, 0.0)
    row = lax.broadcasted_iota(jnp.int32, (rows, rows), 0)
    lane = lax.broadcasted_iota(jnp.int32, (rows, rows), 1)
    earlier = jnp.where(row < lane, 1.0, 0.0).astype(BF16)
    eye = jnp.where(row == lane, 1.0, 0.0).astype(BF16)
    place = jnp.where(member > 0.0, dot(member.astype(BF16), earlier), -1.0)
    for k in range(levels):
        part = slice(k * per, (k + 1) * per)
        meta[z, k] = jnp.concatenate([dense[part], place[part]], axis=0)

    near = jnp.minimum(z, levels - 1 - z)
    sign = jnp.where(2 * z < levels - 1, 1, -1)
    order = []
    for i in range(levels - 1):
        paired = z + sign * (i // 2 + 1) * (1 - 2 * (i % 2))
        order.append(jnp.where(i < 2 * near, paired, z + sign * (i - near + 1)))

    def own_rail(q, d):
        return remote(
            xo.at[c, :, cs(q)],
            xl.at[z, :, cs(q)],
            own_ss.at[d],
            rail_rs.at[z, q],
            beside[d],
            c,
        )

    def own_meta(d):
        return remote(meta.at[z], meta.at[z], mown_ss.at[d], mrail_rs.at[z], beside[d], c)

    def onward(lv):
        up = lv < z
        return jnp.where(up, has[0], has[1]), jnp.where(up, beside[0], beside[1])

    def rail(lv, q):
        return remote(
            xl.at[lv, :, cs(q)],
            xl.at[lv, :, cs(q)],
            rail_ss.at[lv],
            rail_rs.at[lv, q],
            onward(lv)[1],
            c,
        )

    def rail_meta(lv):
        return remote(
            meta.at[lv], meta.at[lv], mrail_ss.at[lv], mrail_rs.at[lv], onward(lv)[1], c
        )

    def deal_meta(lv, d):
        return remote(
            meta.at[lv, z], mall.at[lv, mine], md_ss.at[lv], md_rs.at[lv], *homes[d]
        )

    def met(lv):
        three = mall.at[lv, pl.ds(0, 3)]
        return remote(three, three, md_ss.at[lv], md_rs.at[lv], ep, oc)

    def deal(lv, d, q):
        return remote(
            stage.at[lv, d, :, cs(q)],
            xr.at[lv, mine, :, cs(q)],
            disp_ss.at[lv],
            disp_rs.at[lv],
            *homes[d],
        )

    def dealt(lv):
        return remote(
            stage.at[lv], xr.at[lv, pl.ds(0, 3)], disp_ss.at[lv], disp_rs.at[lv], ep, oc
        )

    def hand(lv, d, s):
        src = (
            res.at[lv, oc, s, x],
            res.at[lv, 0, s, ox],
            res.at[lv, 1, s, ox],
        )[d]
        e, core = ((ep, oc), (across, 0), (across, 1))[d]
        return remote(
            src, ret.at[lv, mine, s], ret_ss.at[lv], ret_rs.at[lv, s], e, core
        )

    def handed(lv, s):
        three = ret.at[lv, pl.ds(0, 3), s]
        return remote(three, three, ret_ss.at[lv], ret_rs.at[lv, s], ep, oc)

    def all_handed(lv):
        three = ret.at[lv, pl.ds(0, 3)]
        return remote(three, three, ret_ss.at[lv], ret_rs.at[lv, 0], ep, oc)

    def back(lv, s, k):
        up = lv > z
        t = jnp.where(up, jnp.minimum(z + 1, levels - 1), jnp.maximum(z - 1, 0))
        slot = jnp.where(up | (lv != t), lv, levels)
        return remote(
            rs_send.at[lv, s, k],
            rs_rx.at[slot, s, k],
            back_ss.at[lv],
            back_rs.at[slot, s, k],
            t * 2 + x,
            c,
        )

    def came(slot, s, k):
        return remote(
            rs_send.at[0, s, k],
            rs_rx.at[slot, s, k],
            back_ss.at[0],
            back_rs.at[slot, s, k],
            ep,
            oc,
        )

    home_x = lambda core: remote(xo.at[core], xo.at[core], ox_ss.at[0], ox_rs.at[0], ep, oc)

    def normalise(part):
        values = tok[part, :].astype(F32)
        scale = lax.rsqrt(jnp.mean(values * values, axis=1, keepdims=True) + 1e-06)
        xo[c, part, :] = (values * scale * gain_ref[...]).astype(BF16)

    with jax.named_scope("tokload"):
        tok_load.wait()
    with jax.named_scope("norm"):
        normalise(pl.ds(0, rows))
    pl.semaphore_wait(barrier, 3 + has[0].astype(jnp.int32) + has[1].astype(jnp.int32))
    for d in range(2):

        @pl.when(has[d])
        def _():
            own_meta(d).start()
            for q in range(CHUNKS):
                own_rail(q, d).start()

    slot_f = lax.broadcasted_iota(jnp.int32, (cap, rows), 0).astype(F32)

    def selection(lv):
        picks = [
            jnp.where(meta[lv, z, pl.ds(per + j, 1), :] == slot_f, 1.0, 0.0)
            for j in (mine, *others)
        ]
        return jnp.concatenate(picks, axis=0).astype(BF16)

    def spread_meta(lv):
        mall[lv, mine] = meta[lv, z]
        for d in range(3):
            deal_meta(lv, d).start()

    def spread(lv, q, pick, block):
        got = dot(pick, block).astype(BF16)
        xr[lv, mine, :, cs(q)] = got[:cap]
        for d in range(3):
            stage[lv, d, :, cs(q)] = got[(d + 1) * cap : (d + 2) * cap]
        for d in (1, 2, 0):
            deal(lv, d, q).start()

    spread_meta(z)
    pick = selection(z)
    for q in range(CHUNKS):
        spread(z, q, pick, xo[c, :, cs(q)])
    home_x(c).start()
    for load in loads:
        load.start()

    def silu_mul(g, u):
        return (g / (1.0 + jnp.exp(-g)) * u).astype(BF16)

    def compute(lv):
        met(lv).wait_recv()
        weight = jnp.concatenate(
            [
                jnp.sum(
                    jnp.where(
                        mall[lv, j, pl.ds(per + mine, 1), :] == slot_f,
                        mall[lv, j, pl.ds(mine, 1), :],
                        0.0,
                    ),
                    axis=1,
                    keepdims=True,
                )
                for j in range(per)
            ],
            axis=0,
        )
        spot = lax.broadcasted_iota(jnp.int32, (rows, per * cap), 1)
        for k in range(2):
            column = lax.dot_general(
                eye,
                mall[lv, 2 * x + k].astype(BF16),
                (((1,), (1,)), ((), ())),
                preferred_element_type=F32,
            ).astype(jnp.int32)
            want = column[:, per : per + 1]
            for j in range(1, per):
                want = jnp.where(spot >= cap * j, column[:, per + j : per + j + 1] + cap * j, want)
            pt[lv, k] = jnp.where(want == spot, 1.0, 0.0).astype(BF16)
        with jax.named_scope("wait_dealt"):
            dealt(lv).wait_recv()
        xs = xr[lv].reshape(per * cap, width)
        hidden = silu_mul(dot(xs, wg[...]), dot(xs, wu[...]))
        for s in range(BACKS):
            for h in range(2):
                out = (dot(hidden, wd[h, :, ss(s)]) * weight).astype(BF16)
                res[lv, h, s] = out.reshape(2, 2 * cap, rw)
            ret[lv, mine, s] = res[lv, c, s, x]

    def send_back(lv, s):
        for d in (1, 2, 0):
            hand(lv, d, s).start()

    def merge(lv, s, k):
        got = jnp.concatenate(
            [ret[lv, j, s, k * cap : (k + 1) * cap, :] for j in range(per)], axis=0
        )
        acc[k] = dot(pt[lv, k], got)

    def add(slot, s, k):
        with jax.named_scope(f"wait_came#s={s}"):
            came(slot, s, k).wait_recv()
        acc[k] += rs_rx[slot, s, k].astype(F32)

    def ready(lv, s):
        with jax.named_scope(f"wait_handed#s={s}"):
            handed(lv, s).wait_recv()

    def give(lv, s):
        ready(lv, s)
        for k in range(2):
            merge(lv, s, k)

            @pl.when(jnp.where(lv > z, has[1], has[0]))
            def _():
                add(lv, s, k)

            rs_send[lv, s, k] = acc[k].astype(BF16)
            back(lv, s, k).start()

    def meet(lv):
        rail_meta(lv).wait_recv()

        @pl.when(onward(lv)[0])
        def _():
            rail_meta(lv).start()

        spread_meta(lv)
        return selection(lv)

    def step(lv, q, pick):
        with jax.named_scope(f"wait_rail#q={q}"):
            rail(lv, q).wait_recv()

        @pl.when(onward(lv)[0])
        def _():
            rail(lv, q).start()

        spread(lv, q, pick, xl[lv, :, cs(q)])

    home_copy = remote(home_send, home_rx, h_ss.at[0], h_rs.at[0], ep, oc)

    def share():
        home_x(oc).wait_recv()
        xs = xo[...].reshape(2 * rows, width)
        shared = silu_mul(dot(xs, sg[...]), dot(xs, su[...]))
        home_send[...] = dot(shared, sd[oc])
        home[...] = dot(shared, sd[c])
        home_copy.start()

    def sent_rails():
        home_x(c).wait_send()
        for d in range(2):

            @pl.when(has[d])
            def _():
                own_meta(d).wait_send()
                remote(xo.at[c], xl.at[z], own_ss.at[d], rail_rs.at[z, 0], ep, oc).wait_send()

        for lv in order:

            @pl.when(onward(lv)[0])
            def _():
                rail_meta(lv).wait_send()
                remote(xl.at[lv], xl.at[lv], rail_ss.at[lv], rail_rs.at[lv, 0], ep, oc).wait_send()

    def sent_deals(lv):
        met(lv).wait_send()
        dealt(lv).wait_send()

    def sent_back(lv):
        all_handed(lv).wait_send()

    near0, near1, near2 = order
    def loaded():
        for load in loads:
            load.wait()

    @pl.when(at_end)
    def _():
        with jax.named_scope("gather0"):
            pick = meet(near0)
            for q in range(CHUNKS):
                step(near0, q, pick)
        pick = meet(near1)
        step(near1, 0, pick)
        step(near1, 1, pick)
        loaded()
        with jax.named_scope("compute0"):
            compute(near0)
        send_back(near0, 0)
        step(near1, 2, pick)
        send_back(near0, 1)
        step(near1, 3, pick)
        send_back(near0, 2)
        pick = meet(near2)
        with jax.named_scope("give0"):
            give(near0, 0)
        with jax.named_scope("share"):
            share()
        step(near2, 0, pick)
        with jax.named_scope("computez"):
            compute(z)
        step(near2, 1, pick)
        with jax.named_scope("give0"):
            give(near0, 1)
        step(near2, 2, pick)
        with jax.named_scope("compute1"):
            compute(near1)
        with jax.named_scope("give0"):
            give(near0, 2)
        step(near2, 3, pick)
        send_back(near1, 0)
        send_back(near1, 1)
        with jax.named_scope("compute2"):
            compute(near2)
        for s in range(BACKS):
            send_back(near2, s)
        send_back(near1, 2)
        send_back(near1, 3)
        send_back(near0, 3)
        for s in range(BACKS):
            send_back(z, s)
        for lv, s in (
            (near1, 0),
            (near1, 1),
            (near2, 0),
            (near2, 1),
            (near2, 2),
            (near2, 3),
            (near1, 2),
            (near1, 3),
            (near0, 3),
        ):
            with jax.named_scope(f"give{0 if lv is near0 else 1 if lv is near1 else 2}#s={s}"):
                give(lv, s)
            if lv is near1 and s == 0:
                with jax.named_scope("sent"):
                    sent_rails()
                    for v in (z, near0, near1):
                        sent_deals(v)
        for lv in order:
            sent_back(lv)
        sent_deals(near2)

    @pl.when(jnp.logical_not(at_end))
    def _():
        for lv in order:
            with jax.named_scope("gather"):
                pick = meet(lv)
                for q in range(CHUNKS):
                    step(lv, q, pick)
        loaded()
        for k, lv in enumerate((near0, near1)):
            with jax.named_scope(f"compute{k}"):
                compute(lv)
            if k == 0:
                for s in range(BACKS):
                    send_back(lv, s)
        with jax.named_scope("share"):
            share()
        with jax.named_scope("computez"):
            compute(z)
        with jax.named_scope("compute2"):
            compute(near2)
        for lv in (near2, near1, z):
            for s in range(BACKS):
                send_back(lv, s)
        with jax.named_scope("sent"):
            sent_rails()
            for lv in (z, *order):
                sent_deals(lv)
            sent_back(near0)
        for lv, s in (
            (near0, 0),
            (near0, 1),
            (near2, 0),
            (near2, 1),
            (near1, 0),
            (near2, 2),
            (near1, 1),
            (near2, 3),
            (near1, 2),
            (near0, 2),
            (near1, 3),
            (near0, 3),
        ):
            with jax.named_scope(f"give{0 if lv is near0 else 1 if lv is near1 else 2}#s={s}"):
                give(lv, s)
        for lv in (near1, near2):
            sent_back(lv)

    home_copy.wait_recv()
    home[...] += home_rx[...]
    square = [jnp.zeros((rows, 1), F32) for _ in range(2)]
    for s in range(BACKS):
        ready(z, s)
        for k in range(2):
            merge(z, s, k)
            for d, slot in ((1, z), (0, levels)):

                @pl.when(has[d])
                def _():
                    add(slot, s, k)

            part = pl.ds(k * rows, rows)
            total = (home[part, ss(s)] + acc[k]).astype(BF16).astype(F32)
            home[part, ss(s)] = total
            square[k] += jnp.sum(total * total, axis=1, keepdims=True)
    for k in range(2):
        sq_send[k * rows : (k + 1) * rows, :] = jnp.broadcast_to(square[k], (rows, 128))
    squares = remote(sq_send, sq_rx, sq_ss.at[0], sq_rs.at[0], ep, oc)
    squares.start()
    with jax.named_scope("wait_sq"):
        squares.wait_recv()
    with jax.named_scope("final"):
      final = lax.rsqrt((sq_send[...] + sq_rx[...])[:, :1] / width + 1e-06)
      out_ref[...] = (home[...] * final * out_gain_ref[c]).astype(BF16)

    with jax.named_scope("sentend"):
        for lv in order:
            remote(rs_send.at[lv], rs_rx.at[lv], back_ss.at[lv], back_rs.at[lv, 0, 0], ep, oc).wait_send()
        sent_back(z)
        home_copy.wait_send()
        squares.wait_send()


def ladder_local(
    n,
    cap,
    tokens,
    expert_ids,
    gate_weights,
    norm_gain,
    expert_gate,
    expert_up,
    expert_down,
    shared_gate,
    shared_up,
    shared_down,
    out_gain,
):
    rows, width = tokens.shape
    ff = expert_gate.shape[2]
    sh = shared_gate.shape[1]
    cols = width // 2
    levels = n // 2
    rw = cols // BACKS
    dma = pltpu.SemaphoreType.DMA
    vmem = pl.BlockSpec(memory_space=pltpu.VMEM)
    hbm = pl.BlockSpec(memory_space=pl.ANY)
    return pl.pallas_call(
        functools.partial(ladder_kernel, n, cap),
        out_shape=pltpu.VMEM((2 * rows, cols), BF16),
        in_specs=[vmem] * 2 + [hbm] + [vmem] * 2 + [hbm] * 6,
        out_specs=vmem,
        scratch_shapes=[
            pltpu.VMEM((rows, width), BF16),
            pltpu.VMEM((2, rows, width), BF16),
            pltpu.VMEM((levels, rows, width), BF16),
            pltpu.VMEM((levels, levels, 8, rows), F32),
            pltpu.VMEM((levels, 4, 8, rows), F32),
            pltpu.VMEM((levels, 3, cap, width), BF16),
            pltpu.VMEM((levels, 4, cap, width), BF16),
            pltpu.VMEM((width, ff), BF16),
            pltpu.VMEM((width, ff), BF16),
            pltpu.VMEM((2, ff, cols), BF16),
            pltpu.VMEM((width, sh), BF16),
            pltpu.VMEM((width, sh), BF16),
            pltpu.VMEM((2, sh, cols), BF16),
            pltpu.VMEM((levels, 2, BACKS, 2, 2 * cap, rw), BF16),
            pltpu.VMEM((levels, 4, BACKS, 2 * cap, rw), BF16),
            pltpu.VMEM((levels, 2, rows, 4 * cap), BF16),
            pltpu.VMEM((2, rows, rw), F32),
            pltpu.VMEM((levels, BACKS, 2, rows, rw), BF16),
            pltpu.VMEM((levels + 1, BACKS, 2, rows, rw), BF16),
            pltpu.VMEM((2 * rows, cols), F32),
            pltpu.VMEM((2 * rows, cols), F32),
            pltpu.VMEM((2 * rows, cols), F32),
            pltpu.VMEM((2 * rows, 128), F32),
            pltpu.VMEM((2 * rows, 128), F32),
            dma((1,)),
            dma((8,)),
            dma((2,)),
            dma((levels,)),
            dma((levels, CHUNKS)),
            dma((2,)),
            dma((levels,)),
            dma((levels,)),
            dma((levels,)),
            dma((levels,)),
            dma((levels,)),
            dma((levels,)),
            dma((levels,)),
            dma((levels, BACKS)),
            dma((levels,)),
            dma((levels + 1, BACKS, 2)),
            dma((1,)),
            dma((1,)),
            dma((1,)),
            dma((1,)),
            dma((1,)),
            dma((1,)),
        ],
        compiler_params=pltpu.CompilerParams(
            collective_id=0, has_side_effects=True, vmem_limit_bytes=60 * 1024 * 1024
        ),
    )(
        expert_ids.T,
        gate_weights.T,
        tokens,
        norm_gain.reshape(1, width),
        out_gain.reshape(2, 1, cols),
        expert_gate,
        expert_up,
        expert_down,
        shared_gate,
        shared_up,
        shared_down,
    )


TOPK = 4


def expert_work(received, expert_gate, expert_up, expert_down):
    gate = jnp.einsum("slcd,ldf->slcf", received, expert_gate, preferred_element_type=jnp.float32)
    upper = jnp.einsum("slcd,ldf->slcf", received, expert_up, preferred_element_type=jnp.float32)
    hidden = (jax.nn.silu(gate) * upper).astype(jnp.bfloat16)
    return jnp.einsum(
        "slcf,lfd->slcd", hidden, expert_down, preferred_element_type=jnp.float32
    ).astype(jnp.bfloat16)


def local(
    tokens,
    expert_ids,
    gate_weights,
    norm_gain,
    expert_gate,
    expert_up,
    expert_down,
    shared_gate,
    shared_up,
    shared_down,
    out_gain,
):
    local_rows = tokens.shape[0]
    width = tokens.shape[1]
    ep_count = lax.axis_size("ep")
    tp_count = lax.axis_size("tp")
    device_count = ep_count * tp_count
    local_experts = expert_gate.shape[0]
    expert_count = device_count * local_experts
    capacity = 3 * local_rows * TOPK // (2 * expert_count)
    values = tokens.astype(jnp.float32)
    scale = lax.rsqrt(jnp.mean(values * values, axis=1, keepdims=True) + 1e-06)
    normed = (values * scale * norm_gain).astype(jnp.bfloat16)
    flat_ids = expert_ids.reshape(-1)
    one_hot = (flat_ids[:, None] == jnp.arange(expert_count, dtype=jnp.int32)[None, :]).astype(
        jnp.int32
    )
    earlier = jnp.cumsum(one_hot, axis=0) - one_hot
    slot_index = jnp.sum(earlier * one_hot, axis=1)
    target = flat_ids * capacity + slot_index
    copy_rows = normed[jnp.arange(local_rows * TOPK, dtype=jnp.int32) // TOPK]
    outgoing = jnp.zeros((expert_count * capacity, width), jnp.bfloat16).at[target].set(copy_rows)
    sending = outgoing.reshape(device_count, local_experts * capacity, width)
    received = lax.all_to_all(sending, ("ep", "tp"), split_axis=0, concat_axis=0, tiled=True)
    received = received.reshape(device_count, local_experts, capacity, width)
    results = expert_work(received, expert_gate, expert_up, expert_down)
    results = results.reshape(device_count, local_experts * capacity, width)
    returned = lax.all_to_all(results, ("ep", "tp"), split_axis=0, concat_axis=0, tiled=True)
    returned = returned.reshape(expert_count * capacity, width)
    picked = returned[target].astype(jnp.float32).reshape(local_rows, TOPK, width)
    routed = jnp.sum(picked * gate_weights[:, :, None], axis=1)
    piece = lax.all_gather(normed, "tp", axis=0, tiled=True)
    gate = jnp.dot(piece, shared_gate, preferred_element_type=jnp.float32)
    upper = jnp.dot(piece, shared_up, preferred_element_type=jnp.float32)
    shared_hidden = (jax.nn.silu(gate) * upper).astype(jnp.bfloat16)
    shared_out = lax.psum_scatter(
        jnp.dot(shared_hidden, shared_down, preferred_element_type=jnp.float32),
        "tp",
        scatter_dimension=0,
        tiled=True,
    )
    mixed = (routed + shared_out).astype(jnp.bfloat16)
    mixed_values = mixed.astype(jnp.float32)
    final_scale = lax.rsqrt(jnp.mean(mixed_values * mixed_values, axis=1, keepdims=True) + 1e-06)
    normalized = (mixed_values * final_scale * out_gain).astype(jnp.bfloat16)
    return lax.all_to_all(normalized, "tp", split_axis=1, concat_axis=0, tiled=True)


def solution(mesh):
    in_specs = (
        P(("grp", "ep", "tp"), None),
        P(("grp", "ep", "tp"), None),
        P(("grp", "ep", "tp"), None),
        P(),
        P(("ep", "tp"), None, None),
        P(("ep", "tp"), None, None),
        P(("ep", "tp"), None, None),
        P(None, "tp"),
        P(None, "tp"),
        P("tp", None),
        P(),
    )
    out_specs = P(("grp", "ep"), "tp")
    n, tp = mesh.shape["ep"], mesh.shape["tp"]

    def run(*args):
        tokens, expert_gate = args[0], args[4]
        rows = tokens.shape[0] // mesh.size
        experts = expert_gate.shape[0]
        cap = 3 * rows * args[1].shape[1] // (2 * experts)
        dense = experts == n * tp and experts <= 8 * args[1].shape[1]
        dense = dense and tp == 2 and n == 8 and rows == 128 and cap % 16 == 0
        body = functools.partial(ladder_local, n, cap) if dense else local
        return jax.shard_map(
            body, mesh=mesh, in_specs=in_specs, out_specs=out_specs, check_vma=False
        )(*args)

    return run
```

time: 92 us -> 81.1 us (0.88)
  Pallas kernels: 90.1 us -> 80.1 us
    pallas_call x1, Pallas kernels: 90.1 us -> 80.1 us  [ladder_local(): pl.pallas_call(functools.partial(ladder_kernel, n, cap), out_shape=pltpu....]
where the time goes in v1:
time: 81.1 us; the launch traced here: 80.9 us
  Pallas kernels  80.1 us (99%)
    pallas_call x1, Pallas kernels, ladder_local(): pl.pallas_call(functools.partial(ladder_kernel, n, cap), out_shape=pltpu....  80.1 us

profile of v1, /device:TPU:9, one launch (start us, length us, event | category | flops | bytes accessed | tf_op | source)
XLA Modules:
  0.0 80.9 jit_solution(2873994302434826688)
XLA Ops:
  0.0 80.1 %shard_map.109 = bf16[256,1024]{1,0:T(8,128)(2,1)S(1)} custom-call(s32[4,128]{1,0:T(4,128)} %bitcast.6, f32[4,128]{1,0:T(4,128)} %bitcast.7, bf16[128,2048]{1,0:T(8,128)(2,1)} %tok_hbm.1, f32[1,2048]{1,0:T(1,128)} %bitcast.4, f32[2,1,1024]{2,1,0:T(1,128)} %bitcast.5, bf16[1,2048,512]{2,1,0:T(8,128)(2,1)} %eg_hbm.1, bf16[1,2048,512]{2,1,0:T(8,128)(2,1)} %eu_hbm.1, ...), custom_call_target="tpu_custom_call" | custom-call | tf_op jit(solution)/shard_map/pallas_call | solution.py:619
  80.1 0.8 copy.13

commit v2 on v1

--- a/solution.py
+++ b/solution.py
@@ -10,6 +10,13 @@
 MESH = pl.DeviceIdType.MESH
 CHUNKS = 4
 BACKS = 4
+
+
+def pieces(s, k, rows):
+    if s < BACKS - 1:
+        return [(2 * s + k, 0, rows)]
+    half = rows // 2
+    return [(2 * s + 2 * k + i, i * half, half) for i in range(2)]
 F32 = jnp.float32
 BF16 = jnp.bfloat16
 
@@ -17,11 +24,11 @@
 def ladder_kernel(
     n,
     cap,
-    ids_ref,
-    gates_ref,
+    ids_hbm,
+    gates_hbm,
     tok_hbm,
-    gain_ref,
-    out_gain_ref,
+    gain_hbm,
+    out_gain_hbm,
     eg_hbm,
     eu_hbm,
     ed_hbm,
@@ -29,6 +36,10 @@
     su_hbm,
     sd_hbm,
     out_ref,
+    ids_ref,
+    gates_ref,
+    gain_ref,
+    out_gain_ref,
     tok,
     xo,
     xl,
@@ -45,6 +56,13 @@
     res,
     ret,
     pt,
+    pc,
+    comb,
+    mallp,
+    rh,
+    ro,
+    cross_tx,
+    cross_rx,
     acc,
     rs_send,
     rs_rx,
@@ -69,6 +87,14 @@
     ret_rs,
     back_ss,
     back_rs,
+    mp_ss,
+    mp_rs,
+    rh_ss,
+    rh_rs,
+    ro_ss,
+    ro_rs,
+    cross_ss,
+    cross_rs,
     ox_ss,
     ox_rs,
     h_ss,
@@ -97,6 +123,12 @@
     beside = (jnp.minimum(ep + 2, n - 1), jnp.maximum(ep - 2, 0))
     at_end = (z == 0) | (z == levels - 1)
 
+    firsts = [(ids_hbm, ids_ref), (gates_hbm, gates_ref), (tok_hbm, tok), (gain_hbm, gain_ref)]
+    firsts.append((out_gain_hbm, out_gain_ref))
+    firsts = [pltpu.make_async_copy(a, b, tok_sem.at[i]) for i, (a, b) in enumerate(firsts)]
+    for load in firsts:
+        load.start()
+
     def signal(e, core):
         pl.semaphore_signal(barrier, inc=1, device_id={"ep": e, "tp": core}, device_id_type=MESH)
 
@@ -108,9 +140,6 @@
         @pl.when(has[d])
         def _():
             signal(beside[d], c)
-
-    tok_load = pltpu.make_async_copy(tok_hbm, tok, tok_sem.at[0])
-    tok_load.start()
 
     loads = [
         (sg_hbm, sg),
@@ -142,6 +171,8 @@
     def ss(s):
         return pl.ds(s * rw, rw)
 
+    for load in firsts[:2]:
+        load.wait()
     expert = lax.broadcasted_iota(jnp.int32, (experts, rows), 0)
     dense = jnp.zeros((experts, rows), F32)
     member = jnp.zeros((experts, rows), F32)
@@ -165,6 +196,9 @@
         paired = z + sign * (i // 2 + 1) * (1 - 2 * (i % 2))
         order.append(jnp.where(i < 2 * near, paired, z + sign * (i - near + 1)))
 
+    pair = z + 1 - 2 * (z % 2)
+    inner = jnp.where(2 * z < levels - 1, levels, z)
+
     def own_rail(q, d):
         return remote(
             xo.at[c, :, cs(q)],
@@ -239,28 +273,56 @@
         three = ret.at[lv, pl.ds(0, 3)]
         return remote(three, three, ret_ss.at[lv], ret_rs.at[lv, 0], ep, oc)
 
-    def back(lv, s, k):
+    def back(lv, s, k, piece):
         up = lv > z
         t = jnp.where(up, jnp.minimum(z + 1, levels - 1), jnp.maximum(z - 1, 0))
         slot = jnp.where(up | (lv != t), lv, levels)
+        i, first, count = piece
         return remote(
-            rs_send.at[lv, s, k],
-            rs_rx.at[slot, s, k],
+            rs_send.at[lv, s, k, pl.ds(first, count)],
+            rs_rx.at[slot, s, k, pl.ds(first, count)],
             back_ss.at[lv],
-            back_rs.at[slot, s, k],
+            back_rs.at[slot, i],
             t * 2 + x,
             c,
         )
 
-    def came(slot, s, k):
+    def deal_pair(d):
         return remote(
-            rs_send.at[0, s, k],
-            rs_rx.at[slot, s, k],
-            back_ss.at[0],
-            back_rs.at[slot, s, k],
-            ep,
-            oc,
-        )
+            meta.at[z, pair], mallp.at[mine], mp_ss.at[0], mp_rs.at[0], *homes[d]
+        )
+
+    def pair_met():
+        three = mallp.at[pl.ds(0, 3)]
+        return remote(three, three, mp_ss.at[0], mp_rs.at[0], ep, oc)
+
+    def hand_pair(lv, s, h, whole):
+        src, dst = res.at[lv, h, s], rh.at[c, s]
+        if not whole:
+            src, dst = src.at[ox], dst.at[ox]
+        return remote(src, dst, rh_ss.at[0], rh_rs.at[s], pair * 2 + x, h)
+
+    def paired(s, whole):
+        both = rh.at[pl.ds(0, 2), s] if whole else rh.at[pl.ds(0, 2), s, 0]
+        return remote(both, both, rh_ss.at[0], rh_rs.at[s], ep, oc)
+
+    def hand_own(s):
+        return remote(res.at[z, oc, s], ro.at[c, s], ro_ss.at[0], ro_rs.at[s], ep, oc)
+
+    def cross_copy(s, k):
+        return remote(
+            cross_tx.at[s, k],
+            cross_rx.at[s, k],
+            cross_ss.at[0],
+            cross_rs.at[s, k],
+            across,
+            c,
+        )
+
+    def came(slot, s, k, piece):
+        i, first, count = piece
+        part = rs_rx.at[slot, s, k, pl.ds(first, count)]
+        return remote(part, part, back_ss.at[0], back_rs.at[slot, i], ep, oc)
 
     home_x = lambda core: remote(xo.at[core], xo.at[core], ox_ss.at[0], ox_rs.at[0], ep, oc)
 
@@ -270,7 +332,8 @@
         xo[c, part, :] = (values * scale * gain_ref[...]).astype(BF16)
 
     with jax.named_scope("tokload"):
-        tok_load.wait()
+        for load in firsts[2:]:
+            load.wait()
     with jax.named_scope("norm"):
         normalise(pl.ds(0, rows))
     pl.semaphore_wait(barrier, 3 + has[0].astype(jnp.int32) + has[1].astype(jnp.int32))
@@ -305,6 +368,9 @@
             deal(lv, d, q).start()
 
     spread_meta(z)
+    mallp[mine] = meta[z, pair]
+    for d in range(3):
+        deal_pair(d).start()
     pick = selection(z)
     for q in range(CHUNKS):
         spread(z, q, pick, xo[c, :, cs(q)])
@@ -315,7 +381,26 @@
     def silu_mul(g, u):
         return (g / (1.0 + jnp.exp(-g)) * u).astype(BF16)
 
-    def compute(lv):
+    def columns(m):
+        return lax.dot_general(
+            eye, m.astype(BF16), (((1,), (1,)), ((), ())), preferred_element_type=F32
+        ).astype(jnp.int32)
+
+    def two(m):
+        col = columns(m)
+        return [
+            jnp.where(x == 0, col[:, per + j : per + j + 1], col[:, per + 2 + j : per + 3 + j])
+            for j in range(2)
+        ]
+
+    def expander(wants):
+        spot = lax.broadcasted_iota(jnp.int32, (rows, len(wants) * cap), 1)
+        want = wants[0]
+        for j in range(1, len(wants)):
+            want = jnp.where(spot >= cap * j, wants[j] + cap * j, want)
+        return jnp.where(want == spot, 1.0, 0.0).astype(BF16)
+
+    def compute(lv, kind):
         met(lv).wait_recv()
         weight = jnp.concatenate(
             [
@@ -332,18 +417,18 @@
             ],
             axis=0,
         )
-        spot = lax.broadcasted_iota(jnp.int32, (rows, per * cap), 1)
         for k in range(2):
-            column = lax.dot_general(
-                eye,
-                mall[lv, 2 * x + k].astype(BF16),
-                (((1,), (1,)), ((), ())),
-                preferred_element_type=F32,
-            ).astype(jnp.int32)
-            want = column[:, per : per + 1]
-            for j in range(1, per):
-                want = jnp.where(spot >= cap * j, column[:, per + j : per + j + 1] + cap * j, want)
-            pt[lv, k] = jnp.where(want == spot, 1.0, 0.0).astype(BF16)
+            if kind == "far":
+                col = columns(mall[lv, 2 * x + k])
+                pt[lv, k] = expander([col[:, per + j : per + j + 1] for j in range(per)])
+            elif kind == "chain":
+                pc[k] = expander(two(mall[lv, 2 * x + k]))
+        if kind == "own":
+            pair_met().wait_recv()
+            for r, rail_x in enumerate((x, ox)):
+                for k in range(2):
+                    j = 2 * rail_x + k
+                    comb[r, k] = expander(two(mall[lv, j]) + two(mallp[j]))
         with jax.named_scope("wait_dealt"):
             dealt(lv).wait_recv()
         xs = xr[lv].reshape(per * cap, width)
@@ -352,7 +437,10 @@
             for h in range(2):
                 out = (dot(hidden, wd[h, :, ss(s)]) * weight).astype(BF16)
                 res[lv, h, s] = out.reshape(2, 2 * cap, rw)
-            ret[lv, mine, s] = res[lv, c, s, x]
+            if kind in ("far", "chain"):
+                ret[lv, mine, s] = res[lv, c, s, x]
+            elif kind == "own":
+                ro[c, s] = res[lv, c, s]
 
     def send_back(lv, s):
         for d in (1, 2, 0):
@@ -364,26 +452,64 @@
         )
         acc[k] = dot(pt[lv, k], got)
 
-    def add(slot, s, k):
+    def add(slot, s, k, piece):
         with jax.named_scope(f"wait_came#s={s}"):
-            came(slot, s, k).wait_recv()
-        acc[k] += rs_rx[slot, s, k].astype(F32)
+            came(slot, s, k, piece).wait_recv()
+        part = pl.ds(piece[1], piece[2])
+        acc[k, part, :] += rs_rx[slot, s, k, part, :].astype(F32)
 
     def ready(lv, s):
         with jax.named_scope(f"wait_handed#s={s}"):
             handed(lv, s).wait_recv()
+
+    def pass_on(lv, s, k, piece):
+        part = pl.ds(piece[1], piece[2])
+        rs_send[lv, s, k, part, :] = acc[k, part, :].astype(BF16)
+        back(lv, s, k, piece).start()
 
     def give(lv, s):
         ready(lv, s)
         for k in range(2):
             merge(lv, s, k)
-
-            @pl.when(jnp.where(lv > z, has[1], has[0]))
-            def _():
-                add(lv, s, k)
-
-            rs_send[lv, s, k] = acc[k].astype(BF16)
-            back(lv, s, k).start()
+            for piece in pieces(s, k, rows):
+
+                @pl.when(jnp.where(lv > z, has[1], has[0]))
+                def _():
+                    add(lv, s, k, piece)
+
+                pass_on(lv, s, k, piece)
+
+    def part_of(ref, j, s, r, k):
+        return ref[j, s, r, k * cap : (k + 1) * cap, :]
+
+    def give_chain(lv, s):
+        one = ret.at[lv, 0, s]
+        remote(one, one, ret_ss.at[lv], ret_rs.at[lv, s], ep, oc).wait_recv()
+        for k in range(2):
+            got = jnp.concatenate(
+                [ret[lv, 2 * x + j, s, k * cap : (k + 1) * cap, :] for j in range(2)], axis=0
+            )
+            acc[k] = dot(pc[k], got)
+            for piece in pieces(s, k, rows):
+                add(lv, s, k, piece)
+                pass_on(lv, s, k, piece)
+
+    def cross(s, whole):
+        hand = remote(ro.at[0, s], ro.at[0, s], ro_ss.at[0], ro_rs.at[s], ep, oc)
+        hand.wait_recv()
+        with jax.named_scope("wait_paired"):
+            paired(s, whole).wait_recv()
+        for k in range(2):
+            got = jnp.concatenate(
+                [part_of(ref, j, s, ox, k) for ref in (ro, rh) for j in range(2)], axis=0
+            )
+            cross_tx[s, k] = dot(comb[1, k], got).astype(BF16)
+            cross_copy(s, k).start()
+
+    def settle(s, k, whole):
+        refs = (ro, rh) if whole else (ro,)
+        got = jnp.concatenate([part_of(ref, j, s, x, k) for ref in refs for j in range(2)], axis=0)
+        acc[k] = dot(comb[0, k, :, : got.shape[0]], got)
 
     def meet(lv):
         rail_meta(lv).wait_recv()
@@ -435,8 +561,16 @@
         met(lv).wait_send()
         dealt(lv).wait_send()
 
-    def sent_back(lv):
-        all_handed(lv).wait_send()
+    def sent_back(lv, lone=False):
+        if lone:
+            one = ret.at[lv, 0]
+            remote(one, one, ret_ss.at[lv], ret_rs.at[lv, 0], ep, oc).wait_send()
+        else:
+            all_handed(lv).wait_send()
+
+    def sent_pair(whole):
+        both = rh.at[pl.ds(0, 2)] if whole else rh.at[0]
+        remote(both, both, rh_ss.at[0], rh_rs.at[0], ep, oc).wait_send()
 
     near0, near1, near2 = order
     def loaded():
@@ -449,64 +583,56 @@
             pick = meet(near0)
             for q in range(CHUNKS):
                 step(near0, q, pick)
+        loaded()
         pick = meet(near1)
         step(near1, 0, pick)
+        with jax.named_scope("computez"):
+            compute(z, "own")
+        for s in range(BACKS):
+            hand_own(s).start()
         step(near1, 1, pick)
-        loaded()
         with jax.named_scope("compute0"):
-            compute(near0)
-        send_back(near0, 0)
+            compute(near0, "pair")
+        for s in range(BACKS):
+            for h in range(2):
+                hand_pair(near0, s, h, True).start()
         step(near1, 2, pick)
-        send_back(near0, 1)
         step(near1, 3, pick)
-        send_back(near0, 2)
         pick = meet(near2)
-        with jax.named_scope("give0"):
-            give(near0, 0)
+        step(near2, 0, pick)
+        with jax.named_scope("compute1"):
+            compute(near1, "far")
+        send_back(near1, 0)
+        step(near2, 1, pick)
         with jax.named_scope("share"):
             share()
-        step(near2, 0, pick)
-        with jax.named_scope("computez"):
-            compute(z)
-        step(near2, 1, pick)
-        with jax.named_scope("give0"):
-            give(near0, 1)
         step(near2, 2, pick)
-        with jax.named_scope("compute1"):
-            compute(near1)
-        with jax.named_scope("give0"):
-            give(near0, 2)
+        with jax.named_scope("give1#s=0"):
+            give(near1, 0)
         step(near2, 3, pick)
-        send_back(near1, 0)
         send_back(near1, 1)
         with jax.named_scope("compute2"):
-            compute(near2)
+            compute(near2, "far")
         for s in range(BACKS):
             send_back(near2, s)
         send_back(near1, 2)
         send_back(near1, 3)
-        send_back(near0, 3)
+        with jax.named_scope("give1#s=1"):
+            give(near1, 1)
+        with jax.named_scope("sent"):
+            sent_rails()
+            for lv in (z, near0, near1):
+                sent_deals(lv)
         for s in range(BACKS):
-            send_back(z, s)
-        for lv, s in (
-            (near1, 0),
-            (near1, 1),
-            (near2, 0),
-            (near2, 1),
-            (near2, 2),
-            (near2, 3),
-            (near1, 2),
-            (near1, 3),
-            (near0, 3),
-        ):
-            with jax.named_scope(f"give{0 if lv is near0 else 1 if lv is near1 else 2}#s={s}"):
-                give(lv, s)
-            if lv is near1 and s == 0:
-                with jax.named_scope("sent"):
-                    sent_rails()
-                    for v in (z, near0, near1):
-                        sent_deals(v)
-        for lv in order:
+            with jax.named_scope(f"give2#s={s}"):
+                give(near2, s)
+            with jax.named_scope(f"cross#s={s}"):
+                cross(s, False)
+        for s in range(2, BACKS):
+            with jax.named_scope(f"give1#s={s}"):
+                give(near1, s)
+        sent_pair(True)
+        for lv in (near1, near2):
             sent_back(lv)
         sent_deals(near2)
 
@@ -518,26 +644,29 @@
                 for q in range(CHUNKS):
                     step(lv, q, pick)
         loaded()
-        for k, lv in enumerate((near0, near1)):
-            with jax.named_scope(f"compute{k}"):
-                compute(lv)
-            if k == 0:
-                for s in range(BACKS):
-                    send_back(lv, s)
+        with jax.named_scope("compute1"):
+            compute(near1, "chain")
+        for s in range(BACKS):
+            for h in range(2):
+                hand_pair(near1, s, h, False).start()
+            hand(near1, 0, s).start()
+        with jax.named_scope("compute0"):
+            compute(near0, "far")
+        for s in range(BACKS):
+            send_back(near0, s)
+        with jax.named_scope("computez"):
+            compute(z, "own")
+        for s in range(BACKS):
+            hand_own(s).start()
         with jax.named_scope("share"):
             share()
-        with jax.named_scope("computez"):
-            compute(z)
         with jax.named_scope("compute2"):
-            compute(near2)
-        for lv in (near2, near1, z):
-            for s in range(BACKS):
-                send_back(lv, s)
-        with jax.named_scope("sent"):
-            sent_rails()
-            for lv in (z, *order):
-                sent_deals(lv)
-            sent_back(near0)
+            compute(near2, "far")
+        for s in range(BACKS):
+            send_back(near2, s)
+        for s in range(BACKS):
+            with jax.named_scope(f"cross#s={s}"):
+                cross(s, True)
         for lv, s in (
             (near0, 0),
             (near0, 1),
@@ -553,23 +682,36 @@
             (near0, 3),
         ):
             with jax.named_scope(f"give{0 if lv is near0 else 1 if lv is near1 else 2}#s={s}"):
-                give(lv, s)
-        for lv in (near1, near2):
-            sent_back(lv)
+                (give_chain if lv is near1 else give)(lv, s)
+            if lv is near0 and s == 0:
+                with jax.named_scope("sent"):
+                    sent_rails()
+                    for v in (z, *order):
+                        sent_deals(v)
+                    sent_back(near0)
+        sent_pair(False)
+        sent_back(near1, True)
+        sent_back(near2)
 
     home_copy.wait_recv()
     home[...] += home_rx[...]
     square = [jnp.zeros((rows, 1), F32) for _ in range(2)]
     for s in range(BACKS):
-        ready(z, s)
         for k in range(2):
-            merge(z, s, k)
-            for d, slot in ((1, z), (0, levels)):
-
-                @pl.when(has[d])
-                def _():
-                    add(slot, s, k)
-
+
+            @pl.when(at_end)
+            def _():
+                settle(s, k, False)
+
+            @pl.when(jnp.logical_not(at_end))
+            def _():
+                settle(s, k, True)
+
+            with jax.named_scope(f"wait_cross#s={s}"):
+                cross_copy(s, k).wait_recv()
+            acc[k] += cross_rx[s, k].astype(F32)
+            for piece in pieces(s, k, rows):
+                add(inner, s, k, piece)
             part = pl.ds(k * rows, rows)
             total = (home[part, ss(s)] + acc[k]).astype(BF16).astype(F32)
             home[part, ss(s)] = total
@@ -585,9 +727,20 @@
       out_ref[...] = (home[...] * final * out_gain_ref[c]).astype(BF16)
 
     with jax.named_scope("sentend"):
-        for lv in order:
-            remote(rs_send.at[lv], rs_rx.at[lv], back_ss.at[lv], back_rs.at[lv, 0, 0], ep, oc).wait_send()
-        sent_back(z)
+        def passed(lv):
+            some = rs_send.at[lv]
+            remote(some, some, back_ss.at[lv], back_rs.at[lv, 0], ep, oc).wait_send()
+
+        for lv in (near1, near2):
+            passed(lv)
+
+        @pl.when(jnp.logical_not(at_end))
+        def _():
+            passed(near0)
+
+        remote(cross_tx, cross_tx, cross_ss.at[0], cross_rs.at[0, 0], ep, oc).wait_send()
+        remote(ro.at[0], ro.at[0], ro_ss.at[0], ro_rs.at[0], ep, oc).wait_send()
+        pair_met().wait_send()
         home_copy.wait_send()
         squares.wait_send()
 
@@ -608,6 +761,7 @@
     out_gain,
 ):
     rows, width = tokens.shape
+    topk = expert_ids.shape[1]
     ff = expert_gate.shape[2]
     sh = shared_gate.shape[1]
     cols = width // 2
@@ -619,9 +773,13 @@
     return pl.pallas_call(
         functools.partial(ladder_kernel, n, cap),
         out_shape=pltpu.VMEM((2 * rows, cols), BF16),
-        in_specs=[vmem] * 2 + [hbm] + [vmem] * 2 + [hbm] * 6,
+        in_specs=[hbm] * 11,
         out_specs=vmem,
         scratch_shapes=[
+            pltpu.VMEM((topk, rows), jnp.int32),
+            pltpu.VMEM((topk, rows), F32),
+            pltpu.VMEM((1, width), F32),
+            pltpu.VMEM((2, 1, cols), F32),
             pltpu.VMEM((rows, width), BF16),
             pltpu.VMEM((2, rows, width), BF16),
             pltpu.VMEM((levels, rows, width), BF16),
@@ -638,6 +796,13 @@
             pltpu.VMEM((levels, 2, BACKS, 2, 2 * cap, rw), BF16),
             pltpu.VMEM((levels, 4, BACKS, 2 * cap, rw), BF16),
             pltpu.VMEM((levels, 2, rows, 4 * cap), BF16),
+            pltpu.VMEM((2, rows, 2 * cap), BF16),
+            pltpu.VMEM((2, 2, rows, 4 * cap), BF16),
+            pltpu.VMEM((4, 8, rows), F32),
+            pltpu.VMEM((2, BACKS, 2, 2 * cap, rw), BF16),
+            pltpu.VMEM((2, BACKS, 2, 2 * cap, rw), BF16),
+            pltpu.VMEM((BACKS, 2, rows, rw), BF16),
+            pltpu.VMEM((BACKS, 2, rows, rw), BF16),
             pltpu.VMEM((2, rows, rw), F32),
             pltpu.VMEM((levels, BACKS, 2, rows, rw), BF16),
             pltpu.VMEM((levels + 1, BACKS, 2, rows, rw), BF16),
@@ -646,7 +811,7 @@
             pltpu.VMEM((2 * rows, cols), F32),
             pltpu.VMEM((2 * rows, 128), F32),
             pltpu.VMEM((2 * rows, 128), F32),
-            dma((1,)),
+            dma((5,)),
             dma((8,)),
             dma((2,)),
             dma((levels,)),
@@ -661,7 +826,15 @@
             dma((levels,)),
             dma((levels, BACKS)),
             dma((levels,)),
-            dma((levels + 1, BACKS, 2)),
+            dma((levels + 1, 2 * BACKS + 2)),
+            dma((1,)),
+            dma((1,)),
+            dma((1,)),
+            dma((BACKS,)),
+            dma((1,)),
+            dma((BACKS,)),
+            dma((1,)),
+            dma((BACKS, 2)),
             dma((1,)),
             dma((1,)),
             dma((1,)),

time: 81.1 us -> 76.9 us (0.948)
  Pallas kernels: 80.1 us -> 75.9 us
    pallas_call x1, Pallas kernels: 80.1 us -> 75.9 us  [ladder_local(): pl.pallas_call(functools.partial(ladder_kernel, n, cap), out_shape=pltpu....]
where the time goes in v2:
time: 76.9 us; the launch traced here: 76.7 us
  Pallas kernels  75.9 us (99%)
  local copies, waits for them, and re-layouts  0.8 us (1%)
    pallas_call x1, Pallas kernels, ladder_local(): pl.pallas_call(functools.partial(ladder_kernel, n, cap), out_shape=pltpu....  75.9 us

profile of v2, /device:TPU:9, one launch (start us, length us, event | category | flops | bytes accessed | tf_op | source)
XLA Modules:
  0.0 76.7 jit_solution(9017728847150766615)
XLA Ops:
  0.0 75.9 %shard_map.109 = bf16[256,1024]{1,0:T(8,128)(2,1)S(1)} custom-call(s32[4,128]{1,0:T(4,128)} %bitcast.6, f32[4,128]{1,0:T(4,128)} %bitcast.7, bf16[128,2048]{1,0:T(8,128)(2,1)} %tok_hbm.1, f32[1,2048]{1,0:T(1,128)} %bitcast.4, f32[2,1,1024]{2,1,0:T(1,128)} %bitcast.5, bf16[1,2048,512]{2,1,0:T(8,128)(2,1)} %eg_hbm.1, bf16[1,2048,512]{2,1,0:T(8,128)(2,1)} %eu_hbm.1, ...), custom_call_target="tpu_custom_call" | custom-call | tf_op jit(solution)/shard_map/pallas_call | solution.py:773
  75.9 0.8 %copy.13 = bf16[256,1024]{1,0:T(8,128)(2,1)} copy(bf16[256,1024]{1,0:T(8,128)(2,1)S(1)} %shard_map.109) | data formatting | bytes 1048576

commit v3 on v2

--- a/solution.py
+++ b/solution.py
@@ -8,7 +8,7 @@
 from jax.sharding import PartitionSpec as P
 
 MESH = pl.DeviceIdType.MESH
-CHUNKS = 4
+CHUNKS = 8
 BACKS = 4
 
 
@@ -197,7 +197,6 @@
         order.append(jnp.where(i < 2 * near, paired, z + sign * (i - near + 1)))
 
     pair = z + 1 - 2 * (z % 2)
-    inner = jnp.where(2 * z < levels - 1, levels, z)
 
     def own_rail(q, d):
         return remote(
@@ -276,13 +275,12 @@
     def back(lv, s, k, piece):
         up = lv > z
         t = jnp.where(up, jnp.minimum(z + 1, levels - 1), jnp.maximum(z - 1, 0))
-        slot = jnp.where(up | (lv != t), lv, levels)
         i, first, count = piece
         return remote(
             rs_send.at[lv, s, k, pl.ds(first, count)],
-            rs_rx.at[slot, s, k, pl.ds(first, count)],
+            rs_rx.at[lv, s, k, pl.ds(first, count)],
             back_ss.at[lv],
-            back_rs.at[slot, i],
+            back_rs.at[lv, i],
             t * 2 + x,
             c,
         )
@@ -521,6 +519,10 @@
         spread_meta(lv)
         return selection(lv)
 
+    def steps(lv, i, pick):
+        for q in range(i * CHUNKS // 4, (i + 1) * CHUNKS // 4):
+            step(lv, q, pick)
+
     def step(lv, q, pick):
         with jax.named_scope(f"wait_rail#q={q}"):
             rail(lv, q).wait_recv()
@@ -585,31 +587,31 @@
                 step(near0, q, pick)
         loaded()
         pick = meet(near1)
-        step(near1, 0, pick)
+        steps(near1, 0, pick)
         with jax.named_scope("computez"):
             compute(z, "own")
         for s in range(BACKS):
             hand_own(s).start()
-        step(near1, 1, pick)
+        steps(near1, 1, pick)
         with jax.named_scope("compute0"):
             compute(near0, "pair")
         for s in range(BACKS):
             for h in range(2):
                 hand_pair(near0, s, h, True).start()
-        step(near1, 2, pick)
-        step(near1, 3, pick)
+        steps(near1, 2, pick)
+        steps(near1, 3, pick)
         pick = meet(near2)
-        step(near2, 0, pick)
+        steps(near2, 0, pick)
         with jax.named_scope("compute1"):
             compute(near1, "far")
         send_back(near1, 0)
-        step(near2, 1, pick)
+        steps(near2, 1, pick)
         with jax.named_scope("share"):
             share()
-        step(near2, 2, pick)
+        steps(near2, 2, pick)
         with jax.named_scope("give1#s=0"):
             give(near1, 0)
-        step(near2, 3, pick)
+        steps(near2, 3, pick)
         send_back(near1, 1)
         with jax.named_scope("compute2"):
             compute(near2, "far")
@@ -711,7 +713,7 @@
                 cross_copy(s, k).wait_recv()
             acc[k] += cross_rx[s, k].astype(F32)
             for piece in pieces(s, k, rows):
-                add(inner, s, k, piece)
+                add(z, s, k, piece)
             part = pl.ds(k * rows, rows)
             total = (home[part, ss(s)] + acc[k]).astype(BF16).astype(F32)
             home[part, ss(s)] = total
@@ -805,7 +807,7 @@
             pltpu.VMEM((BACKS, 2, rows, rw), BF16),
             pltpu.VMEM((2, rows, rw), F32),
             pltpu.VMEM((levels, BACKS, 2, rows, rw), BF16),
-            pltpu.VMEM((levels + 1, BACKS, 2, rows, rw), BF16),
+            pltpu.VMEM((levels, BACKS, 2, rows, rw), BF16),
             pltpu.VMEM((2 * rows, cols), F32),
             pltpu.VMEM((2 * rows, cols), F32),
             pltpu.VMEM((2 * rows, cols), F32),
@@ -826,7 +828,7 @@
             dma((levels,)),
             dma((levels, BACKS)),
             dma((levels,)),
-            dma((levels + 1, 2 * BACKS + 2)),
+            dma((levels, 2 * BACKS + 2)),
             dma((1,)),
             dma((1,)),
             dma((1,)),

time: 76.9 us -> 76.7 us (level); the launches traced: 76.7 us -> 75.5 us
  Pallas kernels: 75.9 us -> 74.7 us
    pallas_call x1, Pallas kernels: 75.9 us -> 74.7 us  [ladder_local(): pl.pallas_call(functools.partial(ladder_kernel, n, cap), out_shape=pltpu....]
where the time goes in v3:
time: 76.7 us; the launch traced here: 75.5 us
  Pallas kernels  74.7 us (97%)
  local copies, waits for them, and re-layouts  0.8 us (1%)
    pallas_call x1, Pallas kernels, ladder_local(): pl.pallas_call(functools.partial(ladder_kernel, n, cap), out_shape=pltpu....  74.7 us

profile of v3, /device:TPU:9, one launch (start us, length us, event | category | flops | bytes accessed | tf_op | source)
XLA Modules:
  0.0 75.5 jit_solution(8567600955743404644)
XLA Ops:
  0.0 74.7 %shard_map.109 = bf16[256,1024]{1,0:T(8,128)(2,1)S(1)} custom-call(s32[4,128]{1,0:T(4,128)} %bitcast.6, f32[4,128]{1,0:T(4,128)} %bitcast.7, bf16[128,2048]{1,0:T(8,128)(2,1)} %tok_hbm.1, f32[1,2048]{1,0:T(1,128)} %bitcast.4, f32[2,1,1024]{2,1,0:T(1,128)} %bitcast.5, bf16[1,2048,512]{2,1,0:T(8,128)(2,1)} %eg_hbm.1, bf16[1,2048,512]{2,1,0:T(8,128)(2,1)} %eu_hbm.1, ...), custom_call_target="tpu_custom_call" | custom-call | tf_op jit(solution)/shard_map/pallas_call | solution.py:775
  74.8 0.8 %copy.13 = bf16[256,1024]{1,0:T(8,128)(2,1)} copy(bf16[256,1024]{1,0:T(8,128)(2,1)S(1)} %shard_map.109) | data formatting | bytes 1048576
